TPU v7x, 256 devices: a whole 4x4x8 slice. The times are simulated.
256 devices in a mesh: kv: 32 (over z, y), tp: 8 (over x, core).
Axes of the slice: x: 4, y: 4, z: 8, core: 2. Of those that a mesh axis runs over, the one named last changes fastest.
Arguments:
- residual_in: bfloat16 [256, 2048], P(None, ('kv', 'tp')), may hold values from -14 to 14
- delta_state: float32 [256, 32, 128, 128], P('kv', 'tp'), may hold values from -1 to 1
- norm_gain_first: float32 [2048], P('kv'), may hold values from 0.1 to 1.9
- gate_first: bfloat16 [2048, 5632], P('kv', 'tp'), may hold values from -0.125 to 0.125
- up_first: bfloat16 [2048, 5632], P('kv', 'tp'), may hold values from -0.125 to 0.125
- down_first: bfloat16 [5632, 2048], P('tp', 'kv'), may hold values from -0.15625 to 0.15625
- norm_gain_mixer: float32 [2048], P('kv'), may hold values from 0.1 to 1.9
- query_weight: bfloat16 [2048, 2048], P('kv', 'tp'), may hold values from -0.125 to 0.125
- key_weight: bfloat16 [2048, 2048], P('kv', 'tp'), may hold values from -0.125 to 0.125
- value_weight: bfloat16 [2048, 4096], P('kv', 'tp'), may hold values from -0.125 to 0.125
- output_gate_weight: bfloat16 [2048, 4096], P('kv', 'tp'), may hold values from -0.125 to 0.125
- beta_weight: bfloat16 [2048, 32], P('kv'), may hold values from -0.125 to 0.125
- decay_weight: bfloat16 [2048, 32], P('kv'), may hold values from -0.125 to 0.125
- decay_rate: float32 [32], P('tp'), may hold values from -2.3 to 1.1
- decay_bias: float32 [32], P('tp'), may hold values from -1 to 1
- head_gain: float32 [128], replicated, may hold values from 0.1 to 1.9
- out_weight: bfloat16 [4096, 2048], P('tp', 'kv'), may hold values from -0.125 to 0.125
- norm_gain_second: float32 [2048], P('kv'), may hold values from 0.1 to 1.9
- gate_second: bfloat16 [2048, 5632], P('kv', 'tp'), may hold values from -0.125 to 0.125
- up_second: bfloat16 [2048, 5632], P('kv', 'tp'), may hold values from -0.125 to 0.125
- down_second: bfloat16 [5632, 2048], P('tp', 'kv'), may hold values from -0.15625 to 0.15625
Outputs:
- residual_out: bfloat16 [256, 2048], P(None, ('kv', 'tp'))
- delta_state_out: float32 [256, 32, 128, 128], P('kv', 'tp')
All inputs are finite; a program needn't handle non-finite values.
Results may differ from a plain program's by a relative error of at most 0.03.
Values may be sent and summed in bfloat16 or wider, within the bound.
A program may use at most 64 MiB of HBM per device.

v0:
```python
import jax
import jax.numpy as jnp
from jax import lax
from jax.sharding import PartitionSpec as P

D = 2048
epsilon = 1e-06


def in_blocks(value, dim, size):
    before, after = (value.shape[:dim], value.shape[dim + 1 :])
    return jnp.moveaxis(value.reshape(*before, size, -1, *after), dim, 0)


def summed_on_arrival(value, axis, dim):
    blocks = in_blocks(value, dim, lax.axis_size(axis))
    arrived = lax.all_to_all(blocks, axis, split_axis=0, concat_axis=0, tiled=True)
    return arrived.astype(jnp.float32).sum(axis=0)


def side_by_side(arrays, axis, dim, along):
    columns = [a.reshape(*a.shape[:along], -1) for a in arrays]
    both = jnp.concatenate(columns, axis=along)
    result, at, outs = (summed_on_arrival(both, axis, dim), 0, [])
    for a, column in zip(arrays, columns):
        piece = result[..., at : at + column.shape[along]]
        outs.append(piece.reshape(*piece.shape[:along], *a.shape[along:]))
        at += column.shape[along]
    return tuple(outs)


def joined_along(blocks, dim):
    dims = list(blocks.shape[1:])
    dims[dim] *= blocks.shape[0]
    return jnp.moveaxis(blocks, 0, dim).reshape(dims)


def from_everyone(value, axis):
    copies = jnp.broadcast_to(value, (lax.axis_size(axis), *value.shape))
    return lax.all_to_all(copies, axis, split_axis=0, concat_axis=0, tiled=True)


def collect(value, axis, dim):
    return joined_along(from_everyone(value, axis), dim)


def activate(summed, square_sums, hidden_cols):
    rowscale = lax.rsqrt(square_sums / D + epsilon)[:, None]
    gate_act = summed[:, :hidden_cols] * rowscale
    up_act = summed[:, hidden_cols:] * rowscale
    return (jax.nn.silu(gate_act) * up_act).astype(jnp.bfloat16)


def feed_forward(residual, norm_gain, gate_weight, up_weight, down_weight, finish):
    as_float = residual.astype(jnp.float32)
    squares = jnp.sum(as_float * as_float, axis=1)
    scaled = (as_float * norm_gain).astype(jnp.bfloat16)
    joined = jnp.concatenate([gate_weight, up_weight], axis=1)
    partial_value = jnp.dot(scaled, joined, preferred_element_type=jnp.float32)
    hidden_cols = gate_weight.shape[1]
    summed, square_sums = side_by_side(
        (partial_value.astype(jnp.bfloat16), squares.astype(jnp.bfloat16)), "kv", 0, 1
    )
    hidden = activate(summed, square_sums, hidden_cols)
    projected = jnp.dot(
        collect(hidden, "kv", 0), down_weight, preferred_element_type=jnp.float32
    ).astype(jnp.bfloat16)
    if finish:
        col_count = residual.shape[1] // lax.axis_size("tp")
        own_cols = lax.dynamic_slice_in_dim(
            as_float, lax.axis_index("tp") * col_count, col_count, 1
        )
        branch = summed_on_arrival(projected, "tp", 1)
        return (own_cols + 0.5 * branch).astype(jnp.bfloat16)
    branch = lax.psum(projected, "tp").astype(jnp.float32)
    return (as_float + 0.5 * branch).astype(jnp.bfloat16)


def unit_heads(projected, head_size):
    activated = jax.nn.silu(projected).reshape(projected.shape[0], -1, head_size)
    return activated * lax.rsqrt(jnp.sum(activated * activated, axis=-1, keepdims=True) + epsilon)


def delta_step(old_state, key_rows, queries, values, beta_gate, decay_gate):
    faded_state = old_state * decay_gate[:, :, None, None]
    predicted = jnp.einsum("rhab,rha->rhb", faded_state, key_rows, precision=lax.Precision.HIGHEST)
    correction = beta_gate[:, :, None] * (values - predicted)
    updated = faded_state + key_rows[:, :, :, None] * correction[:, :, None, :]
    reading = jnp.einsum("rhab,rha->rhb", updated, queries, precision=lax.Precision.HIGHEST)
    return (updated, reading)


def token_mixer(
    residual,
    norm_gain,
    query_weight,
    key_weight,
    value_weight,
    output_gate_weight,
    beta_weight,
    decay_weight,
    decay_rate,
    decay_bias,
    head_gain,
    out_weight,
    old_state,
):
    as_float = residual.astype(jnp.float32)
    squares = jnp.sum(as_float * as_float, axis=1)
    scaled = (as_float * norm_gain).astype(jnp.bfloat16)
    joined = jnp.concatenate([query_weight, key_weight, value_weight, output_gate_weight], axis=1)
    partial_value = jnp.dot(scaled, joined, preferred_element_type=jnp.float32)
    heads_dev = decay_rate.shape[0]
    head_start = lax.axis_index("tp") * heads_dev
    gate_cols = jnp.concatenate(
        [
            lax.dynamic_slice_in_dim(beta_weight, head_start, heads_dev, 1),
            lax.dynamic_slice_in_dim(decay_weight, head_start, heads_dev, 1),
        ],
        axis=1,
    )
    gate_part = jnp.dot(scaled, gate_cols, preferred_element_type=jnp.float32)
    row_count = old_state.shape[0]
    summed, gate_summed, square_sums = side_by_side(
        (
            partial_value.astype(jnp.bfloat16),
            gate_part.astype(jnp.bfloat16),
            squares.astype(jnp.bfloat16),
        ),
        "kv",
        0,
        1,
    )
    rowscale = lax.rsqrt(square_sums / D + epsilon)[:, None]
    summed = summed * rowscale
    gate_summed = gate_summed * rowscale
    head_size = old_state.shape[2]
    key_cols = query_weight.shape[1]
    value_cols = value_weight.shape[1]
    repeat_count = heads_dev // (key_cols // head_size)
    queries = jnp.repeat(
        unit_heads(summed[:, :key_cols], head_size) * head_size ** (-0.5), repeat_count, axis=1
    )
    key_rows = jnp.repeat(
        unit_heads(summed[:, key_cols : 2 * key_cols], head_size), repeat_count, axis=1
    )
    values = jax.nn.silu(summed[:, 2 * key_cols : 2 * key_cols + value_cols]).reshape(
        row_count, heads_dev, head_size
    )
    out_gate = jax.nn.silu(summed[:, 2 * key_cols + value_cols :]).reshape(
        row_count, heads_dev, head_size
    )
    beta_gate = jax.nn.sigmoid(gate_summed[:, :heads_dev])
    decay_gate = jnp.exp(
        -jnp.exp(decay_rate)[None, :]
        * jax.nn.softplus(gate_summed[:, heads_dev:] + decay_bias[None, :])
    )
    new_state, reading = delta_step(old_state, key_rows, queries, values, beta_gate, decay_gate)
    normed = reading * lax.rsqrt(jnp.mean(reading * reading, axis=-1, keepdims=True) + epsilon)
    normed = (
        (normed * head_gain * out_gate)
        .reshape(row_count, heads_dev * head_size)
        .astype(jnp.bfloat16)
    )
    projected = jnp.dot(
        collect(normed, "kv", 0), out_weight, preferred_element_type=jnp.float32
    ).astype(jnp.bfloat16)
    branch = lax.psum(projected, "tp").astype(jnp.float32)
    return ((as_float + branch).astype(jnp.bfloat16), new_state)


def body(
    residual_in,
    delta_state,
    norm_gain_first,
    gate_first,
    up_first,
    down_first,
    norm_gain_mixer,
    query_weight,
    key_weight,
    value_weight,
    output_gate_weight,
    beta_weight,
    decay_weight,
    decay_rate,
    decay_bias,
    head_gain,
    out_weight,
    norm_gain_second,
    gate_second,
    up_second,
    down_second,
):
    columns = lax.all_gather(residual_in, "tp", axis=1, tiled=True)
    after_first = feed_forward(columns, norm_gain_first, gate_first, up_first, down_first, False)
    after_mixer, new_state = token_mixer(
        after_first,
        norm_gain_mixer,
        query_weight,
        key_weight,
        value_weight,
        output_gate_weight,
        beta_weight,
        decay_weight,
        decay_rate,
        decay_bias,
        head_gain,
        out_weight,
        delta_state,
    )
    residual_out = feed_forward(
        after_mixer, norm_gain_second, gate_second, up_second, down_second, True
    )
    return (residual_out, new_state)


def solution(mesh):
    placed = (
        P(None, ("kv", "tp")),
        P("kv", "tp", None, None),
        P("kv"),
        P("kv", "tp"),
        P("kv", "tp"),
        P("tp", "kv"),
        P("kv"),
        P("kv", "tp"),
        P("kv", "tp"),
        P("kv", "tp"),
        P("kv", "tp"),
        P("kv", None),
        P("kv", None),
        P("tp"),
        P("tp"),
        P(),
        P("tp", "kv"),
        P("kv"),
        P("kv", "tp"),
        P("kv", "tp"),
        P("tp", "kv"),
    )
    return jax.shard_map(
        body,
        mesh=mesh,
        in_specs=placed,
        out_specs=(P(None, ("kv", "tp")), P("kv", "tp", None, None)),
        check_vma=False,
    )
```

profile of v0, /device:TPU:1, one launch (start us, length us, event | category | flops | bytes accessed | tf_op | source)
XLA Modules:
  0.0 230.6 jit_solution(4892839816095156955)
XLA Ops:
  0.6 16.2 %all_gather.3 = bf16[256,64]{0,1:T(8,128)(2,1)S(1)} all-gather(bf16[256,8]{0,1:T(8,128)(2,1)} %param.21), channel_id=1, replica_groups=mesh['kv'=32,'tp'=8] {'tp'}, dimensions={1}, use_global_device_ids=true | all-gather | bytes 36864 | tf_op jit(solution)/shard_map/all_gather | solution.py:195
  16.9 0.2 convert_element_type.152
  17.1 1.4 fusion
  18.7 31.4 %all_to_all.35 = bf16[32,8,1409]{2,1,0:T(8,128)(2,1)S(1)} all-to-all(bf16[32,8,1409]{2,1,0:T(8,128)(2,1)S(1)} %pad_maximum_fusion), channel_id=1, replica_groups=mesh['kv'=32,'tp'=8] {'kv'}, dimensions={0} | all-to-all | bytes 1442816 | tf_op jit(solution)/shard_map/all_to_all | solution.py:17
  50.1 0.1 convert_reduce_fusion.2
  50.2 0.1 fusion.57
  50.3 0.1 fusion.36
  50.4 0.8 broadcast_in_dim.10
  51.2 5.6 %all-to-all-start.1 = ((bf16[32,8,704]{2,1,0:T(8,128)(2,1)}), bf16[32,8,704]{2,1,0:T(8,128)(2,1)S(1)}, u32[]{:S(2)}, u32[]{:S(2)}) async-start(bf16[32,8,704]{2,1,0:T(8,128)(2,1)} %broadcast_in_dim.10), calls=%async_computation.1 | async-start | bytes 786432 | tf_op jit(solution)/shard_map/all_to_all | solution.py:40
  56.8 0.7 constant_dynamic-slice_fusion
  57.5 12.1 %all-to-all-done.1 = bf16[32,8,704]{2,1,0:T(8,128)(2,1)S(1)} async-done(((bf16[32,8,704]{2,1,0:T(8,128)(2,1)}), bf16[32,8,704]{2,1,0:T(8,128)(2,1)S(1)}, u32[]{:S(2)}, u32[]{:S(2)}) %all-to-all-start.1) | async-done | bytes 360480 | tf_op jit(solution)/shard_map/all_to_all | solution.py:40
  69.6 0.2 convolution_convert_fusion.5
  69.8 23.5 %psum.14 = bf16[256,64]{0,1:T(8,128)(2,1)S(1)} all-reduce(bf16[256,64]{0,1:T(8,128)(2,1)S(1)} %convolution_convert_fusion.5), channel_id=1, replica_groups=mesh['kv'=32,'tp'=8] {'tp'}, use_global_device_ids=true, to_apply=%region_2.3 | all-reduce | flops 16384 | bytes 65536 | tf_op jit(solution)/shard_map/psum | solution.py:75
  93.4 0.2 convolution_convert_fusion.6
  93.6 0.1 copy.64
  93.7 0.2 convert_element_type.153
  94.0 0.5 fusion.1
  94.5 1.1 concatenate.39
  95.6 4.6 %all-to-all-start.2 = ((bf16[32,8,1545]{2,1,0:T(8,128)(2,1)}), bf16[32,8,1545]{2,1,0:T(8,128)(2,1)S(1)}, u32[]{:S(2)}, u32[]{:S(2)}) async-start(bf16[32,8,1545]{2,1,0:T(8,128)(2,1)} %concatenate.39), calls=%async_computation.2 | async-start | bytes 1703936 | tf_op jit(solution)/shard_map/all_to_all | solution.py:17
  100.3 19.5 %all-to-all-done.2 = bf16[32,8,1545]{2,1,0:T(8,128)(2,1)S(1)} async-done(((bf16[32,8,1545]{2,1,0:T(8,128)(2,1)}), bf16[32,8,1545]{2,1,0:T(8,128)(2,1)S(1)}, u32[]{:S(2)}, u32[]{:S(2)}) %all-to-all-start.2) | async-done | bytes 791072 | tf_op jit(solution)/shard_map/all_to_all | solution.py:17
  119.7 0.1 convert_reduce_fusion
  119.8 0.2 fusion.54
  120.0 0.1 slice_multiply_fusion.7
  120.1 0.1 slice_multiply_fusion
  120.2 0.1 fusion.43
  120.3 0.1 add_divide_fusion
  120.4 0.1 copy.56
  120.5 0.1 fusion.44
  120.6 2.0 fusion.3
  122.7 0.7 multiply_add_fusion
  123.6 1.2 copy-done.2
  124.8 1.9 fusion.67
  126.7 0.1 fusion.38
  126.8 0.1 fusion.46
  126.9 17.3 %all_to_all.36 = bf16[32,8,512]{2,1,0:T(8,128)(2,1)S(1)} all-to-all(bf16[32,8,512]{2,1,0:T(8,128)(2,1)S(1)} %broadcast_in_dim.13), channel_id=1, replica_groups=mesh['kv'=32,'tp'=8] {'kv'}, dimensions={0} | all-to-all | bytes 524288 | tf_op jit(solution)/shard_map/all_to_all | solution.py:40
  144.2 0.2 convolution_convert_fusion.3
  144.4 26.0 %psum.15 = bf16[256,64]{0,1:T(8,128)(2,1)S(1)} all-reduce(bf16[256,64]{0,1:T(8,128)(2,1)S(1)} %convolution_convert_fusion.3), channel_id=1, replica_groups=mesh['kv'=32,'tp'=8] {'tp'}, use_global_device_ids=true, to_apply=%region_8.9 | all-reduce | flops 16384 | bytes 65536 | tf_op jit(solution)/shard_map/psum | solution.py:168
  170.4 0.2 convert_element_type.154
  170.7 0.5 fusion.2
  171.2 22.8 %all_to_all.37 = bf16[32,8,1409]{2,1,0:T(8,128)(2,1)S(1)} all-to-all(bf16[32,8,1409]{2,1,0:T(8,128)(2,1)S(1)} %pad_maximum_fusion.1), channel_id=1, replica_groups=mesh['kv'=32,'tp'=8] {'kv'}, dimensions={0} | all-to-all | bytes 1442816 | tf_op jit(solution)/shard_map/all_to_all | solution.py:17
  194.0 0.1 convert_reduce_fusion.1
  194.1 0.1 fusion.51
  194.2 0.1 fusion.34
  194.4 18.7 %all_to_all.38 = bf16[32,8,704]{2,1,0:T(8,128)(2,1)S(1)} all-to-all(bf16[32,8,704]{2,1,0:T(8,128)(2,1)S(1)} %broadcast_in_dim.14), channel_id=1, replica_groups=mesh['kv'=32,'tp'=8] {'kv'}, dimensions={0} | all-to-all | bytes 720896 | tf_op jit(solution)/shard_map/all_to_all | solution.py:40
  213.1 0.9 fusion.5
  214.0 11.3 %all-to-all-start.6 = ((bf16[8,256,8]{1,2,0:T(8,128)(2,1)}), bf16[8,256,8]{1,2,0:T(8,128)(2,1)S(1)}, u32[]{:S(2)}, u32[]{:S(2)}) async-start(bf16[8,256,8]{1,2,0:T(8,128)(2,1)} %fusion.5), calls=%async_computation.6 | async-start | bytes 65536 | tf_op jit(solution)/shard_map/all_to_all | solution.py:17
  225.2 4.7 %all-to-all-done.6 = bf16[8,256,8]{1,2,0:T(8,128)(2,1)S(1)} async-done(((bf16[8,256,8]{1,2,0:T(8,128)(2,1)}), bf16[8,256,8]{1,2,0:T(8,128)(2,1)S(1)}, u32[]{:S(2)}, u32[]{:S(2)}) %all-to-all-start.6) | async-done | bytes 32800 | tf_op jit(solution)/shard_map/all_to_all | solution.py:17
  230.0 0.6 add_convert_fusion
  (49 shorter events, 0.5 us)
Async XLA Ops:
  0.6 68.9 %copy-start = (bf16[704,64]{0,1:T(8,128)(2,1)S(1)}, bf16[704,64]{0,1:T(8,128)(2,1)}, u32[]{:S(2)}) copy-start(bf16[704,64]{0,1:T(8,128)(2,1)} %param.26) | copy-start | bytes 270340
  18.6 74.8 %copy-start.11 = (f32[64]{0:T(128)S(1)}, f32[64]{0:T(128)}, u32[]{:S(2)}) copy-start(f32[64]{0:T(128)} %param.27) | copy-start | bytes 772
  18.6 75.4 %copy-start.6 = (bf16[64,512]{1,0:T(8,128)(2,1)S(1)}, bf16[64,512]{1,0:T(8,128)(2,1)}, u32[]{:S(2)}) copy-start(bf16[64,512]{1,0:T(8,128)(2,1)} %param.31) | copy-start | bytes 196612
  18.6 75.4 %copy-start.7 = (bf16[64,512]{1,0:T(8,128)(2,1)S(1)}, bf16[64,512]{1,0:T(8,128)(2,1)}, u32[]{:S(2)}) copy-start(bf16[64,512]{1,0:T(8,128)(2,1)} %param.30) | copy-start | bytes 196612
  18.6 75.4 %copy-start.9 = (bf16[64,256]{1,0:T(8,128)(2,1)S(1)}, bf16[64,256]{1,0:T(8,128)(2,1)}, u32[]{:S(2)}) copy-start(bf16[64,256]{1,0:T(8,128)(2,1)} %param.29) | copy-start | bytes 98308
  18.7 75.4 %copy-start.10 = (bf16[64,256]{1,0:T(8,128)(2,1)S(1)}, bf16[64,256]{1,0:T(8,128)(2,1)}, u32[]{:S(2)}) copy-start(bf16[64,256]{1,0:T(8,128)(2,1)} %param.28) | copy-start | bytes 98308
  51.2 18.4 %all-to-all-start.1 = ((bf16[32,8,704]{2,1,0:T(8,128)(2,1)}), bf16[32,8,704]{2,1,0:T(8,128)(2,1)S(1)}, u32[]{:S(2)}, u32[]{:S(2)}) async-start(bf16[32,8,704]{2,1,0:T(8,128)(2,1)} %broadcast_in_dim.10), calls=%async_computation.1 | async-start | bytes 786432 | tf_op jit(solution)/shard_map/all_to_all | solution.py:40
  94.0 6.2 %copy-start.15 = (f32[4]{0:T(128)S(1)}, f32[4]{0:T(128)}, u32[]{:S(2)}) copy-start(f32[4]{0:T(128)} %param.34) | copy-start | bytes 52
  94.5 25.8 %copy-start.14 = (f32[4]{0:T(128)S(1)}, f32[4]{0:T(128)}, u32[]{:S(2)}) copy-start(f32[4]{0:T(128)} %param.35) | copy-start | bytes 52
  94.5 26.1 %copy-start.1 = (f32[8,4,128,128]{3,2,1,0:T(8,128)S(1)}, f32[8,4,128,128]{3,2,1,0:T(8,128)}, u32[]{:S(2)}) copy-start(f32[8,4,128,128]{3,2,1,0:T(8,128)} %param.22) | copy-start | bytes 6291460
  95.6 24.1 %all-to-all-start.2 = ((bf16[32,8,1545]{2,1,0:T(8,128)(2,1)}), bf16[32,8,1545]{2,1,0:T(8,128)(2,1)S(1)}, u32[]{:S(2)}, u32[]{:S(2)}) async-start(bf16[32,8,1545]{2,1,0:T(8,128)(2,1)} %concatenate.39), calls=%async_computation.2 | async-start | bytes 1703936 | tf_op jit(solution)/shard_map/all_to_all | solution.py:17
  123.5 1.3 copy-start.2
  123.5 3.3 %copy-start.13 = (f32[128]{0:T(128)S(1)}, f32[128]{0:T(128)}, u32[]{:S(2)}) copy-start(f32[128]{0:T(128)} %param.36) | copy-start | bytes 1540
  123.5 20.7 %copy-start.8 = (bf16[512,64]{0,1:T(8,128)(2,1)S(1)}, bf16[512,64]{0,1:T(8,128)(2,1)}, u32[]{:S(2)}) copy-start(bf16[512,64]{0,1:T(8,128)(2,1)} %param.37) | copy-start | bytes 196612
  123.5 47.1 %copy-start.3 = (bf16[64,704]{1,0:T(8,128)(2,1)S(1)}, bf16[64,704]{1,0:T(8,128)(2,1)}, u32[]{:S(2)}) copy-start(bf16[64,704]{1,0:T(8,128)(2,1)} %param.40) | copy-start | bytes 270340
  123.5 47.1 %copy-start.4 = (bf16[64,704]{1,0:T(8,128)(2,1)S(1)}, bf16[64,704]{1,0:T(8,128)(2,1)}, u32[]{:S(2)}) copy-start(bf16[64,704]{1,0:T(8,128)(2,1)} %param.39) | copy-start | bytes 270340
  123.5 47.1 %copy-start.12 = (f32[64]{0:T(128)S(1)}, f32[64]{0:T(128)}, u32[]{:S(2)}) copy-start(f32[64]{0:T(128)} %param.38) | copy-start | bytes 772
  171.2 41.9 %copy-start.5 = (bf16[704,64]{0,1:T(8,128)(2,1)S(1)}, bf16[704,64]{0,1:T(8,128)(2,1)}, u32[]{:S(2)}) copy-start(bf16[704,64]{0,1:T(8,128)(2,1)} %param.41) | copy-start | bytes 270340
  214.0 16.0 %all-to-all-start.6 = ((bf16[8,256,8]{1,2,0:T(8,128)(2,1)}), bf16[8,256,8]{1,2,0:T(8,128)(2,1)S(1)}, u32[]{:S(2)}, u32[]{:S(2)}) async-start(bf16[8,256,8]{1,2,0:T(8,128)(2,1)} %fusion.5), calls=%async_computation.6 | async-start | bytes 65536 | tf_op jit(solution)/shard_map/all_to_all | solution.py:17
where the time goes:
time: 231 us
  blocking collectives  156 us (68%)
  waiting for transfers between devices  36.3 us (16%)
  starting transfers between devices  21.5 us (9%)
  matrix products  7.71 us (3%)
  local copies, waits for them, and re-layouts  4.91 us (2%)
  other arithmetic  3.23 us (1%)
    all_to_all x2, blocking collectives, summed_on_arrival(): lax.all_to_all(blocks, axis, split_axis=0, concat_axis=0, tiled=True)  54.2 us
    all_to_all x2, blocking collectives, from_everyone(): return lax.all_to_all(copies, axis, split_axis=0, concat_axis=0, tiled=True)  36 us
    psum x1, blocking collectives, token_mixer(): branch = lax.psum(projected, 'tp').astype(jnp.float32)  26 us
    all_to_all x2, waiting for transfers between devices, summed_on_arrival(): lax.all_to_all(blocks, axis, split_axis=0, concat_axis=0, tiled=True)  24.2 us
    psum x1, blocking collectives, feed_forward(): branch = lax.psum(projected, 'tp').astype(jnp.float32)  23.5 us
    all_gather x1, blocking collectives, body(): columns = lax.all_gather(residual_in, 'tp', axis=1, tiled=True)  16.2 us
    all_to_all x2, starting transfers between devices, summed_on_arrival(): lax.all_to_all(blocks, axis, split_axis=0, concat_axis=0, tiled=True)  15.9 us
    all_to_all x1, waiting for transfers between devices, from_everyone(): return lax.all_to_all(copies, axis, split_axis=0, concat_axis=0, tiled=True)  12.1 us
  transfers between devices with their start and end apart: 3, of which 3 were waited for; matrix products, arithmetic and copies ran while one was open for 0% of the time, Pallas kernels for 0%

commit v1 on v0

--- a/solution.py
+++ b/solution.py
@@ -192,7 +192,7 @@
     up_second,
     down_second,
 ):
-    columns = lax.all_gather(residual_in, "tp", axis=1, tiled=True)
+    columns = jnp.concatenate(lax.all_gather(residual_in, "tp"), axis=1)
     after_first = feed_forward(columns, norm_gain_first, gate_first, up_first, down_first, False)
     after_mixer, new_state = token_mixer(
         after_first,

time: 231 us -> 231 us (level)
  no operation moved by 1% of the time
where the time goes in v1:
time: 231 us
  blocking collectives  156 us (68%)
  waiting for transfers between devices  36.3 us (16%)
  starting transfers between devices  21.5 us (9%)
  matrix products  7.71 us (3%)
  local copies, waits for them, and re-layouts  4.91 us (2%)
  other arithmetic  3.23 us (1%)
    all_to_all x2, blocking collectives, summed_on_arrival(): lax.all_to_all(blocks, axis, split_axis=0, concat_axis=0, tiled=True)  54.2 us
    all_to_all x2, blocking collectives, from_everyone(): return lax.all_to_all(copies, axis, split_axis=0, concat_axis=0, tiled=True)  36 us
    psum x1, blocking collectives, token_mixer(): branch = lax.psum(projected, 'tp').astype(jnp.float32)  26 us
    all_to_all x2, waiting for transfers between devices, summed_on_arrival(): lax.all_to_all(blocks, axis, split_axis=0, concat_axis=0, tiled=True)  24.2 us
    psum x1, blocking collectives, feed_forward(): branch = lax.psum(projected, 'tp').astype(jnp.float32)  23.5 us
    all_gather x1, blocking collectives, body(): columns = jnp.concatenate(lax.all_gather(residual_in, 'tp'), axis=1)  16.2 us
    all_to_all x2, starting transfers between devices, summed_on_arrival(): lax.all_to_all(blocks, axis, split_axis=0, concat_axis=0, tiled=True)  15.9 us
    all_to_all x1, waiting for transfers between devices, from_everyone(): return lax.all_to_all(copies, axis, split_axis=0, concat_axis=0, tiled=True)  12.1 us
  transfers between devices with their start and end apart: 3, of which 3 were waited for; matrix products, arithmetic and copies ran while one was open for 0% of the time, Pallas kernels for 0%

profile of v1, /device:TPU:1, one launch (start us, length us, event | category | flops | bytes accessed | tf_op | source)
XLA Modules:
  0.0 230.6 jit_solution(7465245645543897204)
XLA Ops:
  0.6 16.2 %all-gather = bf16[2048,8]{0,1:T(8,128)(2,1)S(1)} all-gather(bf16[256,8]{0,1:T(8,128)(2,1)} %param.21), channel_id=2, replica_groups=mesh['kv'=32,'tp'=8] {'tp'}, dimensions={0}, use_global_device_ids=true | all-gather | bytes 36864 | tf_op jit(solution)/shard_map/all_gather | solution.py:195
  16.9 0.2 convert_element_type.169
  17.1 1.4 fusion
  18.7 31.4 %all_to_all.35 = bf16[32,8,1409]{2,1,0:T(8,128)(2,1)S(1)} all-to-all(bf16[32,8,1409]{2,1,0:T(8,128)(2,1)S(1)} %pad_maximum_fusion), channel_id=1, replica_groups=mesh['kv'=32,'tp'=8] {'kv'}, dimensions={0} | all-to-all | bytes 1442816 | tf_op jit(solution)/shard_map/all_to_all | solution.py:17
  50.1 0.1 convert_reduce_fusion.2
  50.2 0.1 fusion.59
  50.3 0.1 fusion.38
  50.4 0.8 broadcast_in_dim.10
  51.2 5.6 %all-to-all-start.1 = ((bf16[32,8,704]{2,1,0:T(8,128)(2,1)}), bf16[32,8,704]{2,1,0:T(8,128)(2,1)S(1)}, u32[]{:S(2)}, u32[]{:S(2)}) async-start(bf16[32,8,704]{2,1,0:T(8,128)(2,1)} %broadcast_in_dim.10), calls=%async_computation.1 | async-start | bytes 786432 | tf_op jit(solution)/shard_map/all_to_all | solution.py:40
  56.8 0.7 constant_dynamic-slice_fusion
  57.5 12.1 %all-to-all-done.1 = bf16[32,8,704]{2,1,0:T(8,128)(2,1)S(1)} async-done(((bf16[32,8,704]{2,1,0:T(8,128)(2,1)}), bf16[32,8,704]{2,1,0:T(8,128)(2,1)S(1)}, u32[]{:S(2)}, u32[]{:S(2)}) %all-to-all-start.1) | async-done | bytes 360480 | tf_op jit(solution)/shard_map/all_to_all | solution.py:40
  69.6 0.2 convolution_convert_fusion.5
  69.8 23.5 %psum.14 = bf16[256,64]{0,1:T(8,128)(2,1)S(1)} all-reduce(bf16[256,64]{0,1:T(8,128)(2,1)S(1)} %convolution_convert_fusion.5), channel_id=1, replica_groups=mesh['kv'=32,'tp'=8] {'tp'}, use_global_device_ids=true, to_apply=%region_2.3 | all-reduce | flops 16384 | bytes 65536 | tf_op jit(solution)/shard_map/psum | solution.py:75
  93.4 0.2 convolution_convert_fusion.6
  93.6 0.1 copy.64
  93.7 0.2 convert_element_type.170
  94.0 0.5 fusion.1
  94.5 1.1 concatenate.39
  95.6 4.6 %all-to-all-start.2 = ((bf16[32,8,1545]{2,1,0:T(8,128)(2,1)}), bf16[32,8,1545]{2,1,0:T(8,128)(2,1)S(1)}, u32[]{:S(2)}, u32[]{:S(2)}) async-start(bf16[32,8,1545]{2,1,0:T(8,128)(2,1)} %concatenate.39), calls=%async_computation.2 | async-start | bytes 1703936 | tf_op jit(solution)/shard_map/all_to_all | solution.py:17
  100.3 19.5 %all-to-all-done.2 = bf16[32,8,1545]{2,1,0:T(8,128)(2,1)S(1)} async-done(((bf16[32,8,1545]{2,1,0:T(8,128)(2,1)}), bf16[32,8,1545]{2,1,0:T(8,128)(2,1)S(1)}, u32[]{:S(2)}, u32[]{:S(2)}) %all-to-all-start.2) | async-done | bytes 791072 | tf_op jit(solution)/shard_map/all_to_all | solution.py:17
  119.7 0.1 convert_reduce_fusion
  119.8 0.2 fusion.56
  120.0 0.1 slice_multiply_fusion.7
  120.1 0.1 slice_multiply_fusion
  120.2 0.1 fusion.45
  120.3 0.1 add_divide_fusion
  120.4 0.1 copy.56
  120.5 0.1 fusion.46
  120.6 2.0 fusion.3
  122.7 0.7 multiply_add_fusion
  123.6 1.2 copy-done.2
  124.8 1.9 fusion.69
  126.7 0.1 fusion.40
  126.8 0.1 fusion.48
  126.9 17.3 %all_to_all.36 = bf16[32,8,512]{2,1,0:T(8,128)(2,1)S(1)} all-to-all(bf16[32,8,512]{2,1,0:T(8,128)(2,1)S(1)} %broadcast_in_dim.13), channel_id=1, replica_groups=mesh['kv'=32,'tp'=8] {'kv'}, dimensions={0} | all-to-all | bytes 524288 | tf_op jit(solution)/shard_map/all_to_all | solution.py:40
  144.2 0.2 convolution_convert_fusion.3
  144.4 26.0 %psum.15 = bf16[256,64]{0,1:T(8,128)(2,1)S(1)} all-reduce(bf16[256,64]{0,1:T(8,128)(2,1)S(1)} %convolution_convert_fusion.3), channel_id=1, replica_groups=mesh['kv'=32,'tp'=8] {'tp'}, use_global_device_ids=true, to_apply=%region_8.9 | all-reduce | flops 16384 | bytes 65536 | tf_op jit(solution)/shard_map/psum | solution.py:168
  170.4 0.2 convert_element_type.171
  170.7 0.5 fusion.2
  171.2 22.8 %all_to_all.37 = bf16[32,8,1409]{2,1,0:T(8,128)(2,1)S(1)} all-to-all(bf16[32,8,1409]{2,1,0:T(8,128)(2,1)S(1)} %pad_maximum_fusion.1), channel_id=1, replica_groups=mesh['kv'=32,'tp'=8] {'kv'}, dimensions={0} | all-to-all | bytes 1442816 | tf_op jit(solution)/shard_map/all_to_all | solution.py:17
  194.0 0.1 convert_reduce_fusion.1
  194.1 0.1 fusion.53
  194.2 0.1 fusion.36
  194.4 18.7 %all_to_all.38 = bf16[32,8,704]{2,1,0:T(8,128)(2,1)S(1)} all-to-all(bf16[32,8,704]{2,1,0:T(8,128)(2,1)S(1)} %broadcast_in_dim.14), channel_id=1, replica_groups=mesh['kv'=32,'tp'=8] {'kv'}, dimensions={0} | all-to-all | bytes 720896 | tf_op jit(solution)/shard_map/all_to_all | solution.py:40
  213.1 0.9 fusion.5
  214.0 11.3 %all-to-all-start.6 = ((bf16[8,256,8]{1,2,0:T(8,128)(2,1)}), bf16[8,256,8]{1,2,0:T(8,128)(2,1)S(1)}, u32[]{:S(2)}, u32[]{:S(2)}) async-start(bf16[8,256,8]{1,2,0:T(8,128)(2,1)} %fusion.5), calls=%async_computation.6 | async-start | bytes 65536 | tf_op jit(solution)/shard_map/all_to_all | solution.py:17
  225.2 4.7 %all-to-all-done.6 = bf16[8,256,8]{1,2,0:T(8,128)(2,1)S(1)} async-done(((bf16[8,256,8]{1,2,0:T(8,128)(2,1)}), bf16[8,256,8]{1,2,0:T(8,128)(2,1)S(1)}, u32[]{:S(2)}, u32[]{:S(2)}) %all-to-all-start.6) | async-done | bytes 32800 | tf_op jit(solution)/shard_map/all_to_all | solution.py:17
  230.0 0.6 add_convert_fusion
  (49 shorter events, 0.5 us)
Async XLA Ops:
  0.6 68.9 %copy-start = (bf16[704,64]{0,1:T(8,128)(2,1)S(1)}, bf16[704,64]{0,1:T(8,128)(2,1)}, u32[]{:S(2)}) copy-start(bf16[704,64]{0,1:T(8,128)(2,1)} %param.26) | copy-start | bytes 270340
  18.6 74.8 %copy-start.11 = (f32[64]{0:T(128)S(1)}, f32[64]{0:T(128)}, u32[]{:S(2)}) copy-start(f32[64]{0:T(128)} %param.27) | copy-start | bytes 772
  18.6 75.4 %copy-start.6 = (bf16[64,512]{1,0:T(8,128)(2,1)S(1)}, bf16[64,512]{1,0:T(8,128)(2,1)}, u32[]{:S(2)}) copy-start(bf16[64,512]{1,0:T(8,128)(2,1)} %param.31) | copy-start | bytes 196612
  18.6 75.4 %copy-start.7 = (bf16[64,512]{1,0:T(8,128)(2,1)S(1)}, bf16[64,512]{1,0:T(8,128)(2,1)}, u32[]{:S(2)}) copy-start(bf16[64,512]{1,0:T(8,128)(2,1)} %param.30) | copy-start | bytes 196612
  18.6 75.4 %copy-start.9 = (bf16[64,256]{1,0:T(8,128)(2,1)S(1)}, bf16[64,256]{1,0:T(8,128)(2,1)}, u32[]{:S(2)}) copy-start(bf16[64,256]{1,0:T(8,128)(2,1)} %param.29) | copy-start | bytes 98308
  18.7 75.4 %copy-start.10 = (bf16[64,256]{1,0:T(8,128)(2,1)S(1)}, bf16[64,256]{1,0:T(8,128)(2,1)}, u32[]{:S(2)}) copy-start(bf16[64,256]{1,0:T(8,128)(2,1)} %param.28) | copy-start | bytes 98308
  51.2 18.4 %all-to-all-start.1 = ((bf16[32,8,704]{2,1,0:T(8,128)(2,1)}), bf16[32,8,704]{2,1,0:T(8,128)(2,1)S(1)}, u32[]{:S(2)}, u32[]{:S(2)}) async-start(bf16[32,8,704]{2,1,0:T(8,128)(2,1)} %broadcast_in_dim.10), calls=%async_computation.1 | async-start | bytes 786432 | tf_op jit(solution)/shard_map/all_to_all | solution.py:40
  94.0 6.2 %copy-start.15 = (f32[4]{0:T(128)S(1)}, f32[4]{0:T(128)}, u32[]{:S(2)}) copy-start(f32[4]{0:T(128)} %param.34) | copy-start | bytes 52
  94.5 25.8 %copy-start.14 = (f32[4]{0:T(128)S(1)}, f32[4]{0:T(128)}, u32[]{:S(2)}) copy-start(f32[4]{0:T(128)} %param.35) | copy-start | bytes 52
  94.5 26.1 %copy-start.1 = (f32[8,4,128,128]{3,2,1,0:T(8,128)S(1)}, f32[8,4,128,128]{3,2,1,0:T(8,128)}, u32[]{:S(2)}) copy-start(f32[8,4,128,128]{3,2,1,0:T(8,128)} %param.22) | copy-start | bytes 6291460
  95.6 24.1 %all-to-all-start.2 = ((bf16[32,8,1545]{2,1,0:T(8,128)(2,1)}), bf16[32,8,1545]{2,1,0:T(8,128)(2,1)S(1)}, u32[]{:S(2)}, u32[]{:S(2)}) async-start(bf16[32,8,1545]{2,1,0:T(8,128)(2,1)} %concatenate.39), calls=%async_computation.2 | async-start | bytes 1703936 | tf_op jit(solution)/shard_map/all_to_all | solution.py:17
  123.5 1.3 copy-start.2
  123.5 3.3 %copy-start.13 = (f32[128]{0:T(128)S(1)}, f32[128]{0:T(128)}, u32[]{:S(2)}) copy-start(f32[128]{0:T(128)} %param.36) | copy-start | bytes 1540
  123.5 20.7 %copy-start.8 = (bf16[512,64]{0,1:T(8,128)(2,1)S(1)}, bf16[512,64]{0,1:T(8,128)(2,1)}, u32[]{:S(2)}) copy-start(bf16[512,64]{0,1:T(8,128)(2,1)} %param.37) | copy-start | bytes 196612
  123.5 47.1 %copy-start.3 = (bf16[64,704]{1,0:T(8,128)(2,1)S(1)}, bf16[64,704]{1,0:T(8,128)(2,1)}, u32[]{:S(2)}) copy-start(bf16[64,704]{1,0:T(8,128)(2,1)} %param.40) | copy-start | bytes 270340
  123.5 47.1 %copy-start.4 = (bf16[64,704]{1,0:T(8,128)(2,1)S(1)}, bf16[64,704]{1,0:T(8,128)(2,1)}, u32[]{:S(2)}) copy-start(bf16[64,704]{1,0:T(8,128)(2,1)} %param.39) | copy-start | bytes 270340
  123.5 47.1 %copy-start.12 = (f32[64]{0:T(128)S(1)}, f32[64]{0:T(128)}, u32[]{:S(2)}) copy-start(f32[64]{0:T(128)} %param.38) | copy-start | bytes 772
  171.2 41.9 %copy-start.5 = (bf16[704,64]{0,1:T(8,128)(2,1)S(1)}, bf16[704,64]{0,1:T(8,128)(2,1)}, u32[]{:S(2)}) copy-start(bf16[704,64]{0,1:T(8,128)(2,1)} %param.41) | copy-start | bytes 270340
  214.0 16.0 %all-to-all-start.6 = ((bf16[8,256,8]{1,2,0:T(8,128)(2,1)}), bf16[8,256,8]{1,2,0:T(8,128)(2,1)S(1)}, u32[]{:S(2)}, u32[]{:S(2)}) async-start(bf16[8,256,8]{1,2,0:T(8,128)(2,1)} %fusion.5), calls=%async_computation.6 | async-start | bytes 65536 | tf_op jit(solution)/shard_map/all_to_all | solution.py:17
